TPU v7x, 32 devices: a whole 2x2x4 slice. The times are simulated.
32 devices in a mesh: kv: 4 (over y, x), tp: 8 (over z, core).
Axes of the slice: x: 2, y: 2, z: 4, core: 2. Of those that a mesh axis runs over, the one named last changes fastest.
Arguments:
- resid: bfloat16 [32, 4096], P('tp', 'kv'), may hold values from -35 to 35
- attn_gain: bfloat16 [4096], replicated, may hold values from 0.099609375 to 1.8984375
- w_query_nope: bfloat16 [4096, 8192], P('kv', 'tp'), may hold values from -0.09375 to 0.09375
- w_query_rope: bfloat16 [4096, 4096], P('kv', 'tp'), may hold values from -0.09375 to 0.09375
- w_latent: bfloat16 [4096, 512], P('kv'), may hold values from -0.09375 to 0.09375
- w_key_rope: bfloat16 [4096, 64], replicated, may hold values from -0.09375 to 0.09375
- latent_gain: bfloat16 [512], replicated, may hold values from 0.099609375 to 1.8984375
- key_up: bfloat16 [512, 64, 128], P(None, 'tp'), may hold values from -0.5 to 0.5
- value_up: bfloat16 [512, 64, 128], P(None, 'tp'), may hold values from -0.25 to 0.25
- w_out: bfloat16 [8192, 4096], P('tp', 'kv'), may hold values from -4 to 4
- post_gain: bfloat16 [4096], replicated, may hold values from 0.099609375 to 1.8984375
- mlp_gain: bfloat16 [4096], replicated, may hold values from 0.099609375 to 1.8984375
- w_gate: bfloat16 [4096, 11008], P('kv', 'tp'), may hold values from -3 to 3
- w_up: bfloat16 [4096, 11008], P('kv', 'tp'), may hold values from -3 to 3
- w_down: bfloat16 [11008, 4096], P('tp', 'kv'), may hold values from -0.0546875 to 0.0546875
- cache_latent: bfloat16 [32, 2048, 512], P('tp', 'kv'), may hold values from -6 to 6
- cache_rope_key: bfloat16 [32, 2048, 64], P('tp', 'kv'), may hold values from -740 to 740
Outputs:
- next_resid: bfloat16 [32, 4096], P('tp', 'kv')
- new_latent: bfloat16 [32, 512], P('tp')
- new_rope_key: bfloat16 [32, 64], P('tp')
All inputs are finite; a program needn't handle non-finite values.
Results may differ from a plain program's by a relative error of at most 0.035.
Values may be sent and summed in bfloat16 or wider, within the bound.
A program may use at most 64 MiB of HBM per device.

v0:
```python
import jax
import jax.numpy as jnp
from jax import lax
from jax.sharding import PartitionSpec as P

EPS = 1e-06
THETA = 10000.0


def rotate(vector, position):
    half_width = vector.shape[-1] // 2
    frequency = THETA ** (-jnp.arange(half_width, dtype=jnp.float32) / half_width)
    angles = jnp.asarray(position, jnp.float32) * frequency
    cos_table, sin_table = (jnp.cos(angles), jnp.sin(angles))
    lower_half, upper_half = (vector[..., :half_width], vector[..., half_width:])
    return jnp.concatenate(
        [
            lower_half * cos_table - upper_half * sin_table,
            lower_half * sin_table + upper_half * cos_table,
        ],
        axis=-1,
    )


def body(
    resid,
    attn_gain,
    w_query_nope,
    w_query_rope,
    w_latent,
    w_key_rope,
    latent_gain,
    key_up,
    value_up,
    w_out,
    post_gain,
    mlp_gain,
    w_gate,
    w_up,
    w_down,
    cache_latent,
    cache_rope_key,
):
    kv_count = lax.axis_size("kv")
    kv_index = lax.axis_index("kv")
    tp_index = lax.axis_index("tp")
    own_rows, width_dev = resid.shape
    model_width = width_dev * kv_count
    heads_dev = key_up.shape[1]
    pos_dev = cache_latent.shape[1]
    context = pos_dev * kv_count
    score_scale = (key_up.shape[2] + cache_rope_key.shape[2]) ** (-0.5)
    col_start = kv_index * width_dev
    row_start = tp_index * own_rows

    def block_of(vector):
        return lax.dynamic_slice_in_dim(vector, col_start, width_dev, 0).astype(jnp.float32)[
            None, :
        ]

    gathered = lax.all_gather(resid, "tp", axis=0, tiled=True)
    batch_rows = gathered.shape[0]
    gathered_float = gathered.astype(jnp.float32)
    normed_a = (gathered_float * block_of(attn_gain)).astype(jnp.bfloat16)
    own_normed = lax.dynamic_slice_in_dim(normed_a, row_start, own_rows, 0)
    key_rows = lax.dynamic_slice_in_dim(w_key_rope, col_start, width_dev, 0)
    q_nope_sum, q_rope_sum, latent_sum, key_sum, square_sum = (
        lax.psum(
            jnp.dot(normed_a, w_query_nope, preferred_element_type=jnp.float32).astype(
                jnp.bfloat16
            ),
            "kv",
        ).astype(jnp.float32),
        lax.psum(
            jnp.dot(normed_a, w_query_rope, preferred_element_type=jnp.float32).astype(
                jnp.bfloat16
            ),
            "kv",
        ).astype(jnp.float32),
        lax.psum(
            jnp.dot(own_normed, w_latent, preferred_element_type=jnp.float32).astype(jnp.bfloat16),
            "kv",
        ).astype(jnp.float32),
        lax.psum(
            jnp.dot(own_normed, key_rows, preferred_element_type=jnp.float32).astype(jnp.bfloat16),
            "kv",
        ).astype(jnp.float32),
        lax.psum(
            jnp.sum(gathered_float * gathered_float, axis=1).astype(jnp.bfloat16), "kv"
        ).astype(jnp.float32),
    )
    scale_in = lax.rsqrt(square_sum / model_width + EPS)[:, None]
    own_scale = lax.dynamic_slice_in_dim(scale_in, row_start, own_rows, 0)
    q_nope = (q_nope_sum * scale_in).astype(jnp.bfloat16).reshape(batch_rows, heads_dev, -1)
    q_rope = rotate((q_rope_sum * scale_in).reshape(batch_rows, heads_dev, -1), context).astype(
        jnp.bfloat16
    )
    new_latent = (
        latent_sum
        * lax.rsqrt(jnp.mean(latent_sum * latent_sum, axis=1, keepdims=True) + EPS)
        * latent_gain.astype(jnp.float32)[None, :]
    ).astype(jnp.bfloat16)
    new_rope_key = rotate(key_sum * own_scale, context).astype(jnp.bfloat16)
    q_lat = jnp.einsum("bhd,chd->bhc", q_nope, key_up, preferred_element_type=jnp.float32).astype(
        jnp.bfloat16
    )
    seq_lat, seq_rope = (
        lax.all_to_all(q_lat, "tp", split_axis=0, concat_axis=1, tiled=True),
        lax.all_to_all(q_rope, "tp", split_axis=0, concat_axis=1, tiled=True),
    )
    scores = (
        jnp.einsum("bhc,bpc->bhp", seq_lat, cache_latent, preferred_element_type=jnp.float32)
        + jnp.einsum("bhr,bpr->bhp", seq_rope, cache_rope_key, preferred_element_type=jnp.float32)
    ) * score_scale
    own_score = (
        jnp.einsum("bhc,bc->bh", seq_lat, new_latent, preferred_element_type=jnp.float32)
        + jnp.einsum("bhr,br->bh", seq_rope, new_rope_key, preferred_element_type=jnp.float32)
    ) * score_scale
    local_peak = jnp.maximum(jnp.max(scores, axis=2), own_score)
    peak = lax.pmax(local_peak, "kv")
    probs = jnp.exp(scores - peak[:, :, None])
    own_prob = jnp.exp(own_score - peak)
    totals = lax.psum(jnp.sum(probs, axis=2), "kv") + own_prob
    partial_value = jnp.einsum(
        "bhp,bpc->bhc", probs.astype(jnp.bfloat16), cache_latent, preferred_element_type=jnp.float32
    )
    summed = (
        lax.psum(partial_value.astype(jnp.bfloat16), "kv").astype(jnp.float32)
        + own_prob[:, :, None] * new_latent.astype(jnp.float32)[:, None, :]
    )
    o_lat = (summed / totals[:, :, None]).astype(jnp.bfloat16)
    head_lat = lax.all_to_all(o_lat, "tp", split_axis=1, concat_axis=0, tiled=True)
    o_heads = jnp.einsum(
        "bhc,che->bhe", head_lat, value_up, preferred_element_type=jnp.float32
    ).astype(jnp.bfloat16)
    o_flat = o_heads.reshape(batch_rows, -1)
    attended = lax.psum_scatter(
        jnp.dot(o_flat, w_out, preferred_element_type=jnp.float32).astype(jnp.bfloat16),
        "tp",
        scatter_dimension=0,
        tiled=True,
    ).astype(jnp.float32)
    post_square = lax.psum(jnp.sum(attended * attended, axis=1), "kv")
    post_part = attended * lax.rsqrt(post_square / model_width + EPS)[:, None] * block_of(post_gain)
    resid_mid = (resid.astype(jnp.float32) + post_part).astype(jnp.bfloat16)
    mid_rows = lax.all_gather(resid_mid, "tp", axis=0, tiled=True)
    mid_float = mid_rows.astype(jnp.float32)
    normed_m = (mid_float * block_of(mlp_gain)).astype(jnp.bfloat16)
    gate_part = jnp.dot(normed_m, w_gate, preferred_element_type=jnp.float32)
    up_part = jnp.dot(normed_m, w_up, preferred_element_type=jnp.float32)
    square_part = jnp.sum(mid_float * mid_float, axis=1)
    gate_sum, up_sum, mid_square = (
        lax.psum(gate_part.astype(jnp.bfloat16), "kv").astype(jnp.float32),
        lax.psum(up_part.astype(jnp.bfloat16), "kv").astype(jnp.float32),
        lax.psum(square_part.astype(jnp.bfloat16), "kv").astype(jnp.float32),
    )
    scale_mid = lax.rsqrt(mid_square / model_width + EPS)[:, None]
    hidden = (jax.nn.silu(gate_sum * scale_mid) * (up_sum * scale_mid)).astype(jnp.bfloat16)
    lowered = lax.psum_scatter(
        jnp.dot(hidden, w_down, preferred_element_type=jnp.float32).astype(jnp.bfloat16),
        "tp",
        scatter_dimension=0,
        tiled=True,
    ).astype(jnp.float32)
    next_resid = (resid_mid.astype(jnp.float32) + lowered).astype(jnp.bfloat16)
    return (next_resid, new_latent, new_rope_key)


def solution(mesh):
    return jax.shard_map(
        body,
        mesh=mesh,
        in_specs=(
            P("tp", "kv"),
            P(),
            P("kv", "tp"),
            P("kv", "tp"),
            P("kv", None),
            P(),
            P(),
            P(None, "tp", None),
            P(None, "tp", None),
            P("tp", "kv"),
            P(),
            P(),
            P("kv", "tp"),
            P("kv", "tp"),
            P("tp", "kv"),
            P("tp", "kv", None),
            P("tp", "kv", None),
        ),
        out_specs=(P("tp", "kv"), P("tp", None), P("tp", None)),
        check_vma=False,
    )
```

profile of v0, /device:TPU:0, one launch (start us, length us, event | category | flops | bytes accessed | tf_op | source)
XLA Modules:
  0.0 386.5 jit_solution(13030384441631528125)
XLA Ops:
  7.2 16.0 %all-gather = bf16[8,4,1024]{2,1,0:T(4,128)(2,1)S(1)} all-gather(bf16[1,4,1024]{2,1,0:T(4,128)(2,1)} %bitcast.69), channel_id=1, replica_groups=mesh['kv'=4,'tp'=8] {'tp'}, dimensions={0}, use_global_device_ids=true | all-gather | bytes 73728 | tf_op jit(solution)/shard_map/all_gather | solution.py:61
  23.3 0.7 dynamic-slice_convert_fusion.2
  24.0 0.1 multiply_reduce_fusion.1
  24.1 1.0 convolution_convert_fusion.10
  25.2 1.5 convolution_convert_fusion.9
  26.6 1.5 convolution_convert_fusion.8
  28.1 16.7 %all-reduce.2 = (bf16[32]{0:T(256)(128)(2,1)S(1)}, bf16[32,512]{1,0:T(8,128)(2,1)S(1)}, bf16[4,512]{1,0:T(4,128)(2,1)S(1)}, bf16[4,64]{1,0:T(4,128)(2,1)S(1)}) all-reduce(bf16[32]{0:T(256)(128)(2,1)S(1)} %get-tuple-element.15, bf16[32,512]{1,0:T(8,128)(2,1)S(1)} %convolution_convert_fusion.8, ...), channel_id=1, replica_groups=mesh['kv'=4,'tp'=8] {'kv'}, use_global_device_ids=true, to_apply=%region_2.0 | all-reduce | flops 18720 | bytes 74880 | tf_op jit(solution)/shard_map/psum | solution.py:88
  45.2 0.7 reshape.73
  46.0 4.6 %all-to-all-start.1 = ((bf16[8,2,1024]{2,1,0:T(2,128)(2,1)}), bf16[8,2,1024]{2,1,0:T(2,128)(2,1)S(1)}, u32[]{:S(2)}, u32[]{:S(2)}) async-start(bf16[8,2,1024]{2,1,0:T(2,128)(2,1)} %reshape.73), calls=%async_computation.1 | async-start | bytes 65536 | tf_op jit(solution)/shard_map/all_to_all | solution.py:109
  50.7 2.7 convolution_convert_fusion.7
  53.6 0.1 fusion.32
  53.7 42.1 %all-reduce.10.cloned.1.call-done = bf16[32,1024]{1,0:T(8,128)(2,1)} async-done(((bf16[32,1024]{1,0:T(8,128)(2,1)}), bf16[32,1024]{1,0:T(8,128)(2,1)}) %all-reduce.10.cloned.1.call-update) | async-done | bytes 65552 | tf_op jit(solution)/shard_map/psum | solution.py:68
  95.8 1.8 fusion.1
  97.6 0.9 copy.35
  98.4 4.6 %all-to-all-start = ((bf16[32,8,512]{2,1,0:T(8,128)(2,1)}), bf16[32,8,512]{2,1,0:T(8,128)(2,1)S(1)}, u32[]{:S(2)}, u32[]{:S(2)}) async-start(bf16[32,8,512]{2,1,0:T(8,128)(2,1)} %copy.35), calls=%async_computation | async-start | bytes 524288 | tf_op jit(solution)/shard_map/all_to_all | solution.py:108
  103.2 0.1 reshape.74
  103.3 0.1 fusion.23
  103.5 9.3 %all-to-all-done = bf16[32,8,512]{2,1,0:T(8,128)(2,1)S(1)} async-done(((bf16[32,8,512]{2,1,0:T(8,128)(2,1)}), bf16[32,8,512]{2,1,0:T(8,128)(2,1)S(1)}, u32[]{:S(2)}, u32[]{:S(2)}) %all-to-all-start) | async-done | bytes 262176 | tf_op jit(solution)/shard_map/all_to_all | solution.py:108
  112.7 2.3 fusion.10
  115.1 0.2 fusion.8
  115.3 1.3 fusion.48
  116.5 8.9 %pmax.7 = f32[4,64]{1,0:T(4,128)S(1)} all-reduce(f32[4,64]{1,0:T(4,128)S(1)} %fusion.39), channel_id=1, replica_groups=mesh['kv'=4,'tp'=8] {'kv'}, use_global_device_ids=true, to_apply=%region_8.0 | all-reduce | flops 256 | bytes 2048 | tf_op jit(solution)/shard_map/pmax | solution.py:120
  125.5 2.8 convolution_convert_fusion.2
  128.4 0.2 fusion.5
  128.6 8.9 %psum.83 = f32[4,64]{1,0:T(4,128)S(1)} all-reduce(f32[4,64]{1,0:T(4,128)S(1)} %fusion.5), channel_id=1, replica_groups=mesh['kv'=4,'tp'=8] {'kv'}, use_global_device_ids=true, to_apply=%region_11.0 | all-reduce | flops 256 | bytes 2048 | tf_op jit(solution)/shard_map/psum | solution.py:123
  137.5 32.0 %all-reduce.12.cloned.1.call-done = bf16[4,64,512]{2,1,0:T(8,128)(2,1)} async-done(((bf16[4,64,512]{2,1,0:T(8,128)(2,1)}), bf16[4,64,512]{2,1,0:T(8,128)(2,1)}) %all-reduce.12.cloned.1.call-update) | async-done | bytes 262160 | tf_op jit(solution)/shard_map/psum | solution.py:128
  169.5 1.1 divide_convert_fusion
  170.6 0.2 copy.38
  170.9 14.1 %all_to_all.54 = bf16[4,64,512]{2,0,1:T(4,128)(2,1)S(1)} all-to-all(bf16[4,64,512]{2,0,1:T(4,128)(2,1)S(1)} %copy.38), channel_id=1, replica_groups=mesh['kv'=4,'tp'=8] {'tp'}, dimensions={1} | all-to-all | bytes 524288 | tf_op jit(solution)/shard_map/all_to_all | solution.py:132
  185.2 1.5 fusion.2
  186.7 2.7 convolution_convert_fusion.6
  189.5 0.7 dynamic-slice_convert_fusion.1
  190.2 0.6 dynamic-slice.4
  191.4 50.8 %all-reduce.14.cloned.1.call-done = bf16[32,1024]{1,0:T(8,128)(2,1)} async-done(((bf16[32,1024]{1,0:T(8,128)(2,1)}), bf16[32,1024]{1,0:T(8,128)(2,1)}) %all-reduce.14.cloned.1.call-update) | async-done | bytes 65552
  242.2 0.8 fusion.28
  243.1 0.7 dynamic-slice_convert_fusion
  243.8 9.8 %psum.84 = f32[4]{0:T(128)S(1)} all-reduce(f32[4]{0:T(128)S(1)} %fusion.28), channel_id=1, replica_groups=mesh['kv'=4,'tp'=8] {'kv'}, use_global_device_ids=true, to_apply=%region_14.0 | all-reduce | flops 4 | bytes 32 | tf_op jit(solution)/shard_map/psum | solution.py:143
  253.6 0.8 fusion.31
  254.4 14.0 %all-gather.1 = bf16[8,4,1024]{2,1,0:T(4,128)(2,1)S(1)} all-gather(bf16[1,4,1024]{2,1,0:T(4,128)(2,1)S(1)} %bitcast.68), channel_id=1, replica_groups=mesh['kv'=4,'tp'=8] {'tp'}, dimensions={0}, use_global_device_ids=true | all-gather | bytes 73728 | tf_op jit(solution)/shard_map/all_gather | solution.py:146
  268.4 0.1 multiply_reduce_fusion
  268.5 1.6 convolution_convert_fusion.1
  270.2 1.6 convolution_convert_fusion
  271.8 8.0 %psum.86 = bf16[32]{0:T(256)(128)(2,1)S(1)} all-reduce(bf16[32]{0:T(256)(128)(2,1)S(1)} %multiply_reduce_fusion), channel_id=1, replica_groups=mesh['kv'=4,'tp'=8] {'kv'}, use_global_device_ids=true, to_apply=%region_17.0 | all-reduce | flops 32 | bytes 128 | tf_op jit(solution)/shard_map/psum | solution.py:155
  279.8 40.7 %all-reduce.18.cloned.1.call-done = (bf16[32,1376]{1,0:T(8,128)(2,1)}, bf16[32,1376]{1,0:T(8,128)(2,1)}) async-done(((bf16[32,1376]{1,0:T(8,128)(2,1)}, bf16[32,1376]{1,0:T(8,128)(2,1)}), (bf16[32,1376]{1,0:T(8,128)(2,1)}, bf16[32,1376]{1,0:T(8,128)(2,1)})) %all-reduce.18.cloned.1.call-update) | async-done | bytes 176144 | tf_op jit(solution)/shard_map/psum | solution.py:154
  320.5 3.2 convolution_convert_fusion.5
  323.7 0.6 pad_maximum_fusion.1
  324.4 54.3 %all-reduce.16.cloned.1.call-done = bf16[32,1024]{1,0:T(8,128)(2,1)} async-done(((bf16[32,1024]{1,0:T(8,128)(2,1)}), bf16[32,1024]{1,0:T(8,128)(2,1)}) %all-reduce.16.cloned.1.call-update) | async-done | bytes 65552
  378.6 1.3 add_convert_fusion.1
  (44 shorter events, 1.4 us)
Async XLA Ops:
  7.2 261.3 %copy-start = (bf16[1024,1376]{0,1:T(8,128)(2,1)S(1)}, bf16[1024,1376]{0,1:T(8,128)(2,1)}, u32[]{:S(2)}) copy-start(bf16[1024,1376]{0,1:T(8,128)(2,1)} %param.29) | copy-start | bytes 8454148
  46.0 52.5 %all-to-all-start.1 = ((bf16[8,2,1024]{2,1,0:T(2,128)(2,1)}), bf16[8,2,1024]{2,1,0:T(2,128)(2,1)S(1)}, u32[]{:S(2)}, u32[]{:S(2)}) async-start(bf16[8,2,1024]{2,1,0:T(2,128)(2,1)} %reshape.73), calls=%async_computation.1 | async-start | bytes 65536 | tf_op jit(solution)/shard_map/all_to_all | solution.py:109
  50.6 52.6 %copy-start.4 = (bf16[512]{0:T(512)(128)(2,1)S(1)}, bf16[512]{0:T(512)(128)(2,1)}, u32[]{:S(2)}) copy-start(bf16[512]{0:T(512)(128)(2,1)} %param.23) | copy-start | bytes 3076
  50.6 45.2 %all-reduce.10.cloned.1.call-start = ((), (), s32[]{:S(2)}) async-start(), calls=%async_computation.3 | async-start | bytes 131072 | tf_op jit(solution)/shard_map/psum | solution.py:68
  98.4 14.3 %all-to-all-start = ((bf16[32,8,512]{2,1,0:T(8,128)(2,1)}), bf16[32,8,512]{2,1,0:T(8,128)(2,1)S(1)}, u32[]{:S(2)}, u32[]{:S(2)}) async-start(bf16[32,8,512]{2,1,0:T(8,128)(2,1)} %copy.35), calls=%async_computation | async-start | bytes 524288 | tf_op jit(solution)/shard_map/all_to_all | solution.py:108
  103.0 66.5 %all-reduce.12.cloned.1.call-start = ((), (), s32[]{:S(2)}) async-start(), calls=%async_computation.4 | async-start | bytes 524288 | tf_op jit(solution)/shard_map/psum | solution.py:128
  103.2 13.3 %copy-start.3 = (bf16[4,512]{1,0:T(4,128)(2,1)}, bf16[4,512]{1,0:T(4,128)(2,1)S(1)}, u32[]{:S(2)}) copy-start(bf16[4,512]{1,0:T(4,128)(2,1)S(1)} %get-tuple-element.10) | copy-start | bytes 12292
  128.3 113.9 %all-reduce.14.cloned.1.call-start = ((), (), s32[]{:S(2)}) async-start(), calls=%async_computation.5 | async-start | bytes 131072
  185.1 5.1 %copy-start.5 = (u32[32]{0:T(128)S(1)}, u32[32]{0:T(128)}, u32[]{:S(2)}) copy-start(u32[32]{0:T(128)} %constant.53) | copy-start | bytes 388
  185.1 68.5 %copy-start.2 = (bf16[4,1024]{1,0:T(4,128)(2,1)S(1)}, bf16[4,1024]{1,0:T(4,128)(2,1)}, u32[]{:S(2)}) copy-start(bf16[4,1024]{1,0:T(4,128)(2,1)} %param.17) | copy-start | bytes 24580
  189.4 131.1 %all-reduce.18.cloned.1.call-start = ((), (), s32[]{:S(2)}) async-start(), calls=%async_computation.7 | async-start | bytes 360448 | tf_op jit(solution)/shard_map/psum | solution.py:154
  268.4 1.8 copy-start.1
  279.7 98.9 %all-reduce.16.cloned.1.call-start = ((), (), s32[]{:S(2)}) async-start(), calls=%async_computation.6 | async-start | bytes 131072
Sparse Core Ops, SparseCore 0:
  54.3 41.4 all-reduce.9
  128.4 41.0 all-reduce.11
  189.5 52.6 all-reduce.13
  279.9 40.6 all-reduce.17
  323.9 54.7 all-reduce.15
where the time goes:
time: 388 us; the launch traced here: 386 us
  waiting for transfers between devices  229 us (59%)
  blocking collectives  96.5 us (25%)
  matrix products  25.8 us (7%)
  between operations  14.6 us (4%)
  starting transfers between devices  9.46 us (2%)
  other arithmetic  8.04 us (2%)
    unnamed x7, waiting for transfers between devices  105 us
    psum x1, waiting for transfers between devices, body(): lax.psum(jnp.dot(normed_a, w_query_nope, preferred_element_type=jnp.float...  42.1 us
    psum x1, waiting for transfers between devices, body(): lax.psum(up_part.astype(jnp.bfloat16), 'kv').astype(jnp.float32)  40.7 us
    psum x1, waiting for transfers between devices, body(): lax.psum(partial_value.astype(jnp.bfloat16), 'kv').astype(jnp.float32)  32 us
    psum x1, blocking collectives, body(): lax.psum(jnp.sum(gathered_float * gathered_float, axis=1).astype(jnp.bflo...  16.7 us
    all_gather x1, blocking collectives, body(): gathered = lax.all_gather(resid, 'tp', axis=0, tiled=True)  16 us
    all_to_all x1, blocking collectives, body(): lax.all_to_all(o_lat, 'tp', split_axis=1, concat_axis=0, tiled=True)  14.1 us
    all_gather x1, blocking collectives, body(): mid_rows = lax.all_gather(resid_mid, 'tp', axis=0, tiled=True)  14 us
  transfers between devices with their start and end apart: 7, of which 6 were waited for; matrix products, arithmetic and copies ran while one was open for 2% of the time, Pallas kernels for 0%

commit v1 on v0

--- a/solution.py
+++ b/solution.py
@@ -5,6 +5,12 @@
 
 EPS = 1e-06
 THETA = 10000.0
+
+
+def add_all(value, axis):
+    parts = lax.all_gather(value, axis, axis=0, tiled=False)
+    result = parts.sum(axis=0)
+    return result
 
 
 def rotate(vector, position):
@@ -125,7 +131,7 @@
         "bhp,bpc->bhc", probs.astype(jnp.bfloat16), cache_latent, preferred_element_type=jnp.float32
     )
     summed = (
-        lax.psum(partial_value.astype(jnp.bfloat16), "kv").astype(jnp.float32)
+        add_all(partial_value.astype(jnp.bfloat16), "kv").astype(jnp.float32)
         + own_prob[:, :, None] * new_latent.astype(jnp.float32)[:, None, :]
     )
     o_lat = (summed / totals[:, :, None]).astype(jnp.bfloat16)

time: 388 us -> 372 us (0.959)
  waiting for transfers between devices: 229 us -> 213 us
    psum x1 -> x0, waiting for transfers between devices: 32 us -> none  [body(): lax.psum(partial_value.astype(jnp.bfloat16), 'kv').astype(jnp.float32)]
    all_gather x0 -> x1, waiting for transfers between devices: none -> 15.4 us  [add_all(): parts = lax.all_gather(value, axis, axis=0, tiled=False)]
where the time goes in v1:
time: 372 us; the launch traced here: 371 us
  waiting for transfers between devices  213 us (57%)
  blocking collectives  96.5 us (26%)
  matrix products  25.8 us (7%)
  between operations  14.6 us (4%)
  starting transfers between devices  9.46 us (3%)
  other arithmetic  8.51 us (2%)
    unnamed x7, waiting for transfers between devices  105 us
    psum x1, waiting for transfers between devices, body(): lax.psum(jnp.dot(normed_a, w_query_nope, preferred_element_type=jnp.float...  42.1 us
    psum x1, waiting for transfers between devices, body(): lax.psum(up_part.astype(jnp.bfloat16), 'kv').astype(jnp.float32)  40.7 us
    psum x1, blocking collectives, body(): lax.psum(jnp.sum(gathered_float * gathered_float, axis=1).astype(jnp.bflo...  16.7 us
    all_gather x1, blocking collectives, body(): gathered = lax.all_gather(resid, 'tp', axis=0, tiled=True)  16 us
    all_gather x1, waiting for transfers between devices, add_all(): parts = lax.all_gather(value, axis, axis=0, tiled=False)  15.4 us
    all_to_all x1, blocking collectives, body(): lax.all_to_all(o_lat, 'tp', split_axis=1, concat_axis=0, tiled=True)  14.1 us
    all_gather x1, blocking collectives, body(): mid_rows = lax.all_gather(resid_mid, 'tp', axis=0, tiled=True)  14 us
  transfers between devices with their start and end apart: 7, of which 6 were waited for; matrix products, arithmetic and copies ran while one was open for 2% of the time, Pallas kernels for 0%

profile of v1, /device:TPU:0, one launch (start us, length us, event | category | flops | bytes accessed | tf_op | source)
XLA Modules:
  0.0 370.6 jit_solution(6707170506068403217)
XLA Ops:
  7.2 16.0 %all-gather.1 = bf16[8,4,1024]{2,1,0:T(4,128)(2,1)S(1)} all-gather(bf16[1,4,1024]{2,1,0:T(4,128)(2,1)} %bitcast.71), channel_id=1, replica_groups=mesh['kv'=4,'tp'=8] {'tp'}, dimensions={0}, use_global_device_ids=true | all-gather | bytes 73728 | tf_op jit(solution)/shard_map/all_gather | solution.py:67
  23.3 0.7 dynamic-slice_convert_fusion.2
  24.0 0.1 multiply_reduce_fusion.1
  24.1 1.0 convolution_convert_fusion.10
  25.2 1.5 convolution_convert_fusion.9
  26.6 1.5 convolution_convert_fusion.8
  28.1 16.7 %all-reduce.2 = (bf16[32]{0:T(256)(128)(2,1)S(1)}, bf16[32,512]{1,0:T(8,128)(2,1)S(1)}, bf16[4,512]{1,0:T(4,128)(2,1)S(1)}, bf16[4,64]{1,0:T(4,128)(2,1)S(1)}) all-reduce(bf16[32]{0:T(256)(128)(2,1)S(1)} %get-tuple-element.15, bf16[32,512]{1,0:T(8,128)(2,1)S(1)} %convolution_convert_fusion.8, ...), channel_id=1, replica_groups=mesh['kv'=4,'tp'=8] {'kv'}, use_global_device_ids=true, to_apply=%region_2.0 | all-reduce | flops 18720 | bytes 74880 | tf_op jit(solution)/shard_map/psum | solution.py:94
  45.2 0.7 reshape.74
  46.0 4.6 %all-to-all-start.1 = ((bf16[8,2,1024]{2,1,0:T(2,128)(2,1)}), bf16[8,2,1024]{2,1,0:T(2,128)(2,1)S(1)}, u32[]{:S(2)}, u32[]{:S(2)}) async-start(bf16[8,2,1024]{2,1,0:T(2,128)(2,1)} %reshape.74), calls=%async_computation.1 | async-start | bytes 65536 | tf_op jit(solution)/shard_map/all_to_all | solution.py:115
  50.7 2.7 convolution_convert_fusion.7
  53.7 42.1 %all-reduce.9.cloned.1.call-done = bf16[32,1024]{1,0:T(8,128)(2,1)} async-done(((bf16[32,1024]{1,0:T(8,128)(2,1)}), bf16[32,1024]{1,0:T(8,128)(2,1)}) %all-reduce.9.cloned.1.call-update) | async-done | bytes 65552 | tf_op jit(solution)/shard_map/psum | solution.py:74
  95.8 1.8 fusion.1
  97.6 0.9 copy.45
  98.4 4.6 %all-to-all-start = ((bf16[32,8,512]{2,1,0:T(8,128)(2,1)}), bf16[32,8,512]{2,1,0:T(8,128)(2,1)S(1)}, u32[]{:S(2)}, u32[]{:S(2)}) async-start(bf16[32,8,512]{2,1,0:T(8,128)(2,1)} %copy.45), calls=%async_computation | async-start | bytes 524288 | tf_op jit(solution)/shard_map/all_to_all | solution.py:114
  103.3 0.1 fusion.23
  103.5 9.3 %all-to-all-done = bf16[32,8,512]{2,1,0:T(8,128)(2,1)S(1)} async-done(((bf16[32,8,512]{2,1,0:T(8,128)(2,1)}), bf16[32,8,512]{2,1,0:T(8,128)(2,1)S(1)}, u32[]{:S(2)}, u32[]{:S(2)}) %all-to-all-start) | async-done | bytes 262176 | tf_op jit(solution)/shard_map/all_to_all | solution.py:114
  112.7 2.3 fusion.10
  115.1 0.2 fusion.8
  115.3 1.3 fusion.48
  116.5 8.9 %pmax.7 = f32[4,64]{1,0:T(4,128)S(1)} all-reduce(f32[4,64]{1,0:T(4,128)S(1)} %fusion.39), channel_id=1, replica_groups=mesh['kv'=4,'tp'=8] {'kv'}, use_global_device_ids=true, to_apply=%region_8.0 | all-reduce | flops 256 | bytes 2048 | tf_op jit(solution)/shard_map/pmax | solution.py:126
  125.5 2.8 convolution_convert_fusion.2
  128.4 0.2 fusion.5
  128.6 8.9 %psum.75 = f32[4,64]{1,0:T(4,128)S(1)} all-reduce(f32[4,64]{1,0:T(4,128)S(1)} %fusion.5), channel_id=1, replica_groups=mesh['kv'=4,'tp'=8] {'kv'}, use_global_device_ids=true, to_apply=%region_11.0 | all-reduce | flops 256 | bytes 2048 | tf_op jit(solution)/shard_map/psum | solution.py:129
  137.5 15.4 %all-gather.5.cloned.1.call-done = bf16[16,64,512]{2,1,0:T(8,128)(2,1)} async-done(((bf16[4,64,512]{2,1,0:T(8,128)(2,1)}), bf16[16,64,512]{2,1,0:T(8,128)(2,1)}) %all-gather.5.cloned.1.call-update) | async-done | bytes 1048592 | tf_op jit(solution)/shard_map/all_gather | solution.py:11
  152.9 1.4 reduce_sum.59
  154.4 0.2 divide_convert_fusion
  154.5 0.2 copy.48
  154.7 14.1 %all_to_all.54 = bf16[4,64,512]{2,0,1:T(4,128)(2,1)S(1)} all-to-all(bf16[4,64,512]{2,0,1:T(4,128)(2,1)S(1)} %copy.48), channel_id=1, replica_groups=mesh['kv'=4,'tp'=8] {'tp'}, dimensions={1} | all-to-all | bytes 524288 | tf_op jit(solution)/shard_map/all_to_all | solution.py:138
  168.9 0.2 copy.50
  169.2 1.5 fusion.2
  170.8 2.7 convolution_convert_fusion.6
  173.5 0.7 dynamic-slice_convert_fusion.1
  174.2 0.6 dynamic-slice.4
  175.5 50.9 %all-reduce.11.cloned.1.call-done = bf16[32,1024]{1,0:T(8,128)(2,1)} async-done(((bf16[32,1024]{1,0:T(8,128)(2,1)}), bf16[32,1024]{1,0:T(8,128)(2,1)}) %all-reduce.11.cloned.1.call-update) | async-done | bytes 65552
  226.4 0.8 fusion.28
  227.2 0.7 dynamic-slice_convert_fusion
  227.9 9.8 %psum.76 = f32[4]{0:T(128)S(1)} all-reduce(f32[4]{0:T(128)S(1)} %fusion.28), channel_id=1, replica_groups=mesh['kv'=4,'tp'=8] {'kv'}, use_global_device_ids=true, to_apply=%region_14.0 | all-reduce | flops 4 | bytes 32 | tf_op jit(solution)/shard_map/psum | solution.py:149
  237.7 0.8 fusion.31
  238.5 14.0 %all-gather.2 = bf16[8,4,1024]{2,1,0:T(4,128)(2,1)S(1)} all-gather(bf16[1,4,1024]{2,1,0:T(4,128)(2,1)S(1)} %bitcast.70), channel_id=1, replica_groups=mesh['kv'=4,'tp'=8] {'tp'}, dimensions={0}, use_global_device_ids=true | all-gather | bytes 73728 | tf_op jit(solution)/shard_map/all_gather | solution.py:152
  252.5 0.1 multiply_reduce_fusion
  252.6 1.6 convolution_convert_fusion.1
  254.3 1.6 convolution_convert_fusion
  255.9 8.0 %psum.78 = bf16[32]{0:T(256)(128)(2,1)S(1)} all-reduce(bf16[32]{0:T(256)(128)(2,1)S(1)} %multiply_reduce_fusion), channel_id=1, replica_groups=mesh['kv'=4,'tp'=8] {'kv'}, use_global_device_ids=true, to_apply=%region_17.0 | all-reduce | flops 32 | bytes 128 | tf_op jit(solution)/shard_map/psum | solution.py:161
  263.9 40.7 %all-reduce.15.cloned.1.call-done = (bf16[32,1376]{1,0:T(8,128)(2,1)}, bf16[32,1376]{1,0:T(8,128)(2,1)}) async-done(((bf16[32,1376]{1,0:T(8,128)(2,1)}, bf16[32,1376]{1,0:T(8,128)(2,1)}), (bf16[32,1376]{1,0:T(8,128)(2,1)}, bf16[32,1376]{1,0:T(8,128)(2,1)})) %all-reduce.15.cloned.1.call-update) | async-done | bytes 176144 | tf_op jit(solution)/shard_map/psum | solution.py:160
  304.7 3.2 convolution_convert_fusion.5
  307.9 0.6 pad_maximum_fusion.1
  308.5 54.3 %all-reduce.13.cloned.1.call-done = bf16[32,1024]{1,0:T(8,128)(2,1)} async-done(((bf16[32,1024]{1,0:T(8,128)(2,1)}), bf16[32,1024]{1,0:T(8,128)(2,1)}) %all-reduce.13.cloned.1.call-update) | async-done | bytes 65552
  362.8 1.3 add_convert_fusion.1
  (46 shorter events, 1.6 us)
Async XLA Ops:
  7.2 245.5 %copy-start = (bf16[1024,1376]{0,1:T(8,128)(2,1)S(1)}, bf16[1024,1376]{0,1:T(8,128)(2,1)}, u32[]{:S(2)}) copy-start(bf16[1024,1376]{0,1:T(8,128)(2,1)} %param.29) | copy-start | bytes 8454148
  46.0 52.5 %all-to-all-start.1 = ((bf16[8,2,1024]{2,1,0:T(2,128)(2,1)}), bf16[8,2,1024]{2,1,0:T(2,128)(2,1)S(1)}, u32[]{:S(2)}, u32[]{:S(2)}) async-start(bf16[8,2,1024]{2,1,0:T(2,128)(2,1)} %reshape.74), calls=%async_computation.1 | async-start | bytes 65536 | tf_op jit(solution)/shard_map/all_to_all | solution.py:115
  50.6 52.6 %copy-start.4 = (bf16[512]{0:T(512)(128)(2,1)S(1)}, bf16[512]{0:T(512)(128)(2,1)}, u32[]{:S(2)}) copy-start(bf16[512]{0:T(512)(128)(2,1)} %param.23) | copy-start | bytes 3076
  50.6 45.2 %all-reduce.9.cloned.1.call-start = ((), (), s32[]{:S(2)}) async-start(), calls=%async_computation.3 | async-start | bytes 131072 | tf_op jit(solution)/shard_map/psum | solution.py:74
  98.4 14.3 %all-to-all-start = ((bf16[32,8,512]{2,1,0:T(8,128)(2,1)}), bf16[32,8,512]{2,1,0:T(8,128)(2,1)S(1)}, u32[]{:S(2)}, u32[]{:S(2)}) async-start(bf16[32,8,512]{2,1,0:T(8,128)(2,1)} %copy.45), calls=%async_computation | async-start | bytes 524288 | tf_op jit(solution)/shard_map/all_to_all | solution.py:114
  103.0 49.9 %all-gather.5.cloned.1.call-start = ((), (), s32[]{:S(2)}) async-start(), calls=%async_computation.4 | async-start | bytes 1310720 | tf_op jit(solution)/shard_map/all_gather | solution.py:11
  103.2 13.3 %copy-start.3 = (bf16[4,512]{1,0:T(4,128)(2,1)}, bf16[4,512]{1,0:T(4,128)(2,1)S(1)}, u32[]{:S(2)}) copy-start(bf16[4,512]{1,0:T(4,128)(2,1)S(1)} %get-tuple-element.10) | copy-start | bytes 12292
  128.3 98.0 %all-reduce.11.cloned.1.call-start = ((), (), s32[]{:S(2)}) async-start(), calls=%async_computation.5 | async-start | bytes 131072
  169.1 5.1 %copy-start.5 = (u32[32]{0:T(128)S(1)}, u32[32]{0:T(128)}, u32[]{:S(2)}) copy-start(u32[32]{0:T(128)} %constant.55) | copy-start | bytes 388
  169.1 68.6 %copy-start.2 = (bf16[4,1024]{1,0:T(4,128)(2,1)S(1)}, bf16[4,1024]{1,0:T(4,128)(2,1)}, u32[]{:S(2)}) copy-start(bf16[4,1024]{1,0:T(4,128)(2,1)} %param.17) | copy-start | bytes 24580
  173.5 131.2 %all-reduce.15.cloned.1.call-start = ((), (), s32[]{:S(2)}) async-start(), calls=%async_computation.7 | async-start | bytes 360448 | tf_op jit(solution)/shard_map/psum | solution.py:160
  252.5 1.8 copy-start.1
  263.9 98.9 %all-reduce.13.cloned.1.call-start = ((), (), s32[]{:S(2)}) async-start(), calls=%async_computation.6 | async-start | bytes 131072
Sparse Core Ops, SparseCore 0:
  54.3 41.4 all-reduce.8
  128.4 24.4 all-gather.4
  173.6 52.7 all-reduce.10
  264.0 40.6 all-reduce.14
  308.0 54.7 all-reduce.12
